TPU v7x, 32 devices: a whole 2x2x4 slice. The times are simulated.
32 devices in a mesh: fs: 8 (over z, x), tp: 4 (over y, core).
Axes of the slice: x: 2, y: 2, z: 4, core: 2. Of those that a mesh axis runs over, the one named last changes fastest.
Arguments:
- late_input: bfloat16 [4096, 2048], P(('fs', 'tp')), may hold values from -6 to 6
- norm_gain: bfloat16 [2048], replicated, may hold values from 0.099609375 to 1.8984375
- gate_weight: bfloat16 [2048, 2816], P('fs', 'tp'), may hold values from -0.125 to 0.125
- up_weight: bfloat16 [2048, 2816], P('fs', 'tp'), may hold values from -0.125 to 0.125
- down_weight: bfloat16 [2048, 2816], P('fs', 'tp'), may hold values from -0.109375 to 0.109375
- early_input: bfloat16 [4096, 2048], P(('fs', 'tp')), may hold values from -6 to 6
- cotangent: bfloat16 [4096, 2048], P(('fs', 'tp')), may hold values from -6 to 6
- gate_sum: float32 [2048, 2816], P('fs', 'tp'), may hold values from -192 to 192
- up_sum: float32 [2048, 2816], P('fs', 'tp'), may hold values from -192 to 192
- down_sum: float32 [2048, 2816], P('fs', 'tp'), may hold values from -192 to 192
- gain_sum: float32 [2048], replicated, may hold values from -192 to 192
Outputs:
- late_out: bfloat16 [4096, 2048], P(('fs', 'tp'))
- early_grad: bfloat16 [4096, 2048], P(('fs', 'tp'))
- gate_sum_out: float32 [2048, 2816], P('fs', 'tp')
- up_sum_out: float32 [2048, 2816], P('fs', 'tp')
- down_sum_out: float32 [2048, 2816], P('fs', 'tp')
- gain_sum_out: float32 [2048], replicated
All inputs are finite; a program needn't handle non-finite values.
Results may differ from a plain program's by a relative error of at most 0.008.
Values may be sent and summed in bfloat16 or wider, within the bound.
A program may use at most 128 MiB of HBM per device.

v0:
```python
import jax
import jax.numpy as jnp
from jax import lax
from jax.sharding import PartitionSpec as P

epsilon = 1e-05


def normalize(source, gain_f):
    values = source.astype(jnp.float32)
    scale = lax.rsqrt(jnp.mean(values * values, axis=-1, keepdims=True) + epsilon)
    return ((values * scale * gain_f).astype(jnp.bfloat16), scale, values)


def times_transposed(left, right):
    return lax.dot_general(
        left, right, (((1,), (1,)), ((), ())), preferred_element_type=jnp.float32
    )


def column_product(left, right):
    return lax.dot_general(
        left, right, (((0,), (0,)), ((), ())), preferred_element_type=jnp.float32
    )


def per_device(
    late_input,
    norm_gain,
    gate_weight,
    up_weight,
    down_weight,
    early_input,
    cotangent,
    gate_sum,
    up_sum,
    down_sum,
    gain_sum,
):
    gate_whole, up_whole, down_whole = (
        lax.all_gather(gate_weight, "fs", axis=0, tiled=True),
        lax.all_gather(up_weight, "fs", axis=0, tiled=True),
        lax.all_gather(down_weight, "fs", axis=0, tiled=True),
    )
    gain_f = norm_gain.astype(jnp.float32)
    width = gate_weight.shape[1]
    normed, scale, values = normalize(late_input, gain_f)
    piece = lax.all_gather(normed, "tp", axis=0, tiled=True)
    gate = jnp.dot(piece, gate_whole, preferred_element_type=jnp.float32)
    upper = jnp.dot(piece, up_whole, preferred_element_type=jnp.float32)
    hidden = (jax.nn.silu(gate) * upper).astype(jnp.bfloat16)
    mixed = lax.psum_scatter(
        times_transposed(hidden, down_whole).astype(jnp.bfloat16),
        "tp",
        scatter_dimension=0,
        tiled=True,
    ).astype(jnp.float32)
    late_out = (values + 0.5 * mixed).astype(jnp.bfloat16)
    normed_e, scale_e, values_e = normalize(early_input, gain_f)
    normed_all = lax.all_gather(normed_e, "tp", axis=0, tiled=True)
    cot_all = lax.all_gather(cotangent, "tp", axis=0, tiled=True)
    gate_e = jnp.dot(normed_all, gate_whole, preferred_element_type=jnp.float32)
    upper_e = jnp.dot(normed_all, up_whole, preferred_element_type=jnp.float32)
    sigma_e = jax.nn.sigmoid(gate_e)
    hidden_e = (gate_e * sigma_e * upper_e).astype(jnp.bfloat16)
    d_hidden = 0.5 * jnp.dot(cot_all, down_whole, preferred_element_type=jnp.float32)
    d_gate = (d_hidden * upper_e * sigma_e * (1.0 + gate_e * (1.0 - sigma_e))).astype(jnp.bfloat16)
    d_up = (d_hidden * gate_e * sigma_e).astype(jnp.bfloat16)
    d_normed = lax.psum_scatter(
        (times_transposed(d_gate, gate_whole) + times_transposed(d_up, up_whole)).astype(
            jnp.bfloat16
        ),
        "tp",
        scatter_dimension=0,
        tiled=True,
    ).astype(jnp.float32)
    scaled_grad = d_normed * gain_f
    early_grad = (
        cotangent.astype(jnp.float32)
        + scale_e * scaled_grad
        - values_e * scale_e**3 * jnp.mean(values_e * scaled_grad, axis=-1, keepdims=True)
    ).astype(jnp.bfloat16)
    gain_part = jnp.sum(d_normed * values_e * scale_e, axis=0)
    gain_sum_out = gain_sum + lax.psum(gain_part, ("fs", "tp"))
    summed = lax.psum_scatter(
        jnp.concatenate(
            [
                column_product(normed_all, d_gate),
                column_product(normed_all, d_up),
                0.5 * column_product(cot_all, hidden_e),
            ],
            axis=1,
        ),
        "fs",
        scatter_dimension=0,
        tiled=True,
    )
    gate_grad = summed[:, :width]
    up_grad = summed[:, width : 2 * width]
    down_grad = summed[:, 2 * width :]
    early_grad, gate_sum_out, up_sum_out, down_sum_out, gain_sum_out = (
        early_grad,
        gate_sum + gate_grad,
        up_sum + up_grad,
        down_sum + down_grad,
        gain_sum_out,
    )
    return (late_out, early_grad, gate_sum_out, up_sum_out, down_sum_out, gain_sum_out)


def solution(mesh):
    placed = (
        P(("fs", "tp"), None),
        P(),
        P("fs", "tp"),
        P("fs", "tp"),
        P("fs", "tp"),
        P(("fs", "tp"), None),
        P(("fs", "tp"), None),
        P("fs", "tp"),
        P("fs", "tp"),
        P("fs", "tp"),
        P(),
    )
    return jax.shard_map(
        per_device,
        mesh=mesh,
        in_specs=placed,
        out_specs=(
            P(("fs", "tp"), None),
            P(("fs", "tp"), None),
            P("fs", "tp"),
            P("fs", "tp"),
            P("fs", "tp"),
            P(),
        ),
        check_vma=False,
    )
```

profile of v0, /device:TPU:0, one launch (start us, length us, event | category | flops | bytes accessed | tf_op | source)
XLA Modules:
  0.0 657.0 jit_solution(9303688887401447348)
XLA Ops:
  7.2 0.0 all-gather.17.cloned.1.call-start
  7.2 1.2 fusion.9
  8.5 0.7 convert_element_type.49
  9.1 2.0 fusion.11
  11.2 0.0 all-gather.17.cloned.1.call-update
  11.2 0.0 all-gather.9.cloned.1.call-start
  11.2 0.7 all-gather.9.cloned.1.call-update
  11.9 0.0 all-gather.11.cloned.1.call-start
  12.0 0.7 all-gather.11.cloned.1.call-update
  12.7 0.0 all-gather.15.cloned.1.call-start
  12.7 0.5 all-gather.15.cloned.1.call-update
  13.3 0.0 all-gather.13.cloned.1.call-start
  13.3 0.5 all-gather.13.cloned.1.call-update
  13.8 0.0 reduce-scatter.6.cloned.1.call-start
  13.9 22.7 %all-gather.17.cloned.1.call-done = bf16[512,2048]{1,0:T(8,128)(2,1)} async-done(((bf16[128,2048]{1,0:T(8,128)(2,1)}), bf16[512,2048]{1,0:T(8,128)(2,1)}) %all-gather.17.cloned.1.call-update) | async-done | bytes 2097168 | tf_op jit(solution)/shard_map/all_gather | solution.py:60
  36.6 61.6 %all-gather.9.cloned.1.call-done = bf16[2048,704]{0,1:T(8,128)(2,1)} async-done(((bf16[256,704]{0,1:T(8,128)(2,1)}), bf16[2048,704]{0,1:T(8,128)(2,1)}) %all-gather.9.cloned.1.call-update) | async-done | bytes 2883600 | tf_op jit(solution)/shard_map/all_gather | solution.py:41
  98.3 5.2 fusion.21
  103.5 54.6 %all-gather.11.cloned.1.call-done = bf16[2048,704]{0,1:T(8,128)(2,1)} async-done(((bf16[256,704]{0,1:T(8,128)(2,1)}), bf16[2048,704]{0,1:T(8,128)(2,1)}) %all-gather.11.cloned.1.call-update) | async-done | bytes 2883600 | tf_op jit(solution)/shard_map/all_gather | solution.py:42
  158.1 0.0 copy-done.1
  158.1 4.6 fusion.20
  162.7 17.6 %all-gather.15.cloned.1.call-done = bf16[512,2048]{1,0:T(8,128)(2,1)} async-done(((bf16[128,2048]{1,0:T(8,128)(2,1)}), bf16[512,2048]{1,0:T(8,128)(2,1)}) %all-gather.15.cloned.1.call-update) | async-done | bytes 2097168 | tf_op jit(solution)/shard_map/all_gather | solution.py:61
  180.3 61.5 %all-gather.13.cloned.1.call-done = bf16[2048,704]{0,1:T(8,128)(2,1)} async-done(((bf16[256,704]{0,1:T(8,128)(2,1)}), bf16[2048,704]{0,1:T(8,128)(2,1)}) %all-gather.13.cloned.1.call-update) | async-done | bytes 2883600 | tf_op jit(solution)/shard_map/all_gather | solution.py:43
  241.8 5.5 multiply_convert_fusion.1
  247.3 0.0 copy-start.3
  247.3 0.0 copy-start.6
  247.3 0.0 copy-done.5
  247.4 0.0 copy-start.12
  247.4 1.8 fusion.22
  249.2 0.0 copy-done.3
  249.2 0.0 copy-done.6
  249.2 0.5 copy-done.12
  249.7 3.4 add_convert_fusion
  253.1 0.0 reduce-scatter.6.cloned.1.call-update
  253.1 0.0 all-gather.7.cloned.1.call-start
  253.1 1.0 copy-done.2
  254.1 0.2 fusion.5
  254.3 28.3 %reduce-scatter.6.cloned.1.call-done = bf16[128,2048]{1,0:T(8,128)(2,1)} async-done(((bf16[512,2048]{1,0:T(8,128)(2,1)}), bf16[128,2048]{1,0:T(8,128)(2,1)}) %reduce-scatter.6.cloned.1.call-update) | async-done | bytes 524304 | tf_op jit(solution)/shard_map/reduce_scatter | solution.py:69
  282.6 0.0 copy-done
  282.6 1.4 fusion.15
  284.0 2.7 fusion.4
  286.6 0.0 all-gather.7.cloned.1.call-update
  286.7 0.2 reduce-scatter.4.cloned.1.call-start
  286.9 22.5 %all-gather.7.cloned.1.call-done = bf16[512,2048]{1,0:T(8,128)(2,1)} async-done(((bf16[128,2048]{1,0:T(8,128)(2,1)}), bf16[512,2048]{1,0:T(8,128)(2,1)}) %all-gather.7.cloned.1.call-update) | async-done | bytes 2097168 | tf_op jit(solution)/shard_map/all_gather | solution.py:48
  309.4 5.2 fusion.19
  314.6 8.6 %convolution_convert_fusion = bf16[512,2048]{1,0:T(8,128)(2,1)} fusion(bf16[2048,704]{0,1:T(8,128)(2,1)} %all-gather.13.cloned.1.call-done, bf16[512,2048]{1,0:T(8,128)(2,1)} %all-gather.7.cloned.1.call-done, bf16[2048,704]{0,1:T(8,128)(2,1)} %all-gather.11.cloned.1.call-done, f32[512,704]{0,1:T(8,128)} %fusion.19), kind=kOutput, calls=%fused_computation.3 | convolution fusion | flops 2956001280 | bytes 11403264 | tf_op jit(solution)/shard_map/dot_general | solution.py:16
  323.2 0.0 reduce-scatter.4.cloned.1.call-update
  323.2 0.0 reduce-scatter.8.cloned.1.call-start
  323.3 1.0 copy-done.7
  324.3 1.7 fusion.24
  325.9 0.0 copy-done.4
  326.0 1.7 fusion.23
  327.7 0.3 copy-done.14
  328.0 0.4 copy-done.15
  328.4 1.7 multiply_bitcast_fusion
  330.1 6.6 pad_maximum_fusion
  336.7 0.0 reduce-scatter.8.cloned.1.call-update
  336.7 0.0 copy-start.8
  336.7 0.0 copy-start.9
  336.7 40.6 %psum.7 = f32[2048]{0:T(1024)S(1)} all-reduce(f32[2048]{0:T(1024)S(1)} %get-tuple-element.6), channel_id=1, replica_groups=mesh['fs'=8,'tp'=4] {'fs','tp'}, use_global_device_ids=true, to_apply=%region_7.8 | all-reduce | flops 2048 | bytes 16384 | tf_op jit(solution)/shard_map/psum | solution.py:84
  377.3 0.6 add.69
  377.9 2.0 fusion.8
  379.9 267.6 %reduce-scatter.8.cloned.1.call-done = f32[256,2112]{0,1:T(8,128)} async-done(((f32[2048,2112]{0,1:T(8,128)}), f32[256,2112]{0,1:T(8,128)}) %reduce-scatter.8.cloned.1.call-update) | async-done | bytes 2162704 | tf_op jit(solution)/shard_map/reduce_scatter | solution.py:85
  647.5 0.0 copy-done.10
  647.5 3.0 slice_add_fusion
  (19 shorter events, 0.1 us)
Async XLA Ops:
  7.2 29.5 %all-gather.17.cloned.1.call-start = ((), (), s32[]{:S(2)}) async-start(), calls=%async_computation.9 | async-start | bytes 2621440 | tf_op jit(solution)/shard_map/all_gather | solution.py:60
  11.2 87.1 %all-gather.9.cloned.1.call-start = ((), (), s32[]{:S(2)}) async-start(), calls=%async_computation.4 | async-start | bytes 3244032 | tf_op jit(solution)/shard_map/all_gather | solution.py:41
  11.9 146.1 %all-gather.11.cloned.1.call-start = ((), (), s32[]{:S(2)}) async-start(), calls=%async_computation.5 | async-start | bytes 3244032 | tf_op jit(solution)/shard_map/all_gather | solution.py:42
  12.7 167.6 %all-gather.15.cloned.1.call-start = ((), (), s32[]{:S(2)}) async-start(), calls=%async_computation.8 | async-start | bytes 2621440 | tf_op jit(solution)/shard_map/all_gather | solution.py:61
  13.3 228.5 %all-gather.13.cloned.1.call-start = ((), (), s32[]{:S(2)}) async-start(), calls=%async_computation.6 | async-start | bytes 3244032 | tf_op jit(solution)/shard_map/all_gather | solution.py:43
  13.8 268.8 %reduce-scatter.6.cloned.1.call-start = ((), (), s32[]{:S(2)}) async-start(), calls=%async_computation.10 | async-start | bytes 2621440 | tf_op jit(solution)/shard_map/reduce_scatter | solution.py:69
  36.6 121.5 %copy-start.1 = (bf16[512,2048]{1,0:T(8,128)(2,1)S(1)}, bf16[512,2048]{1,0:T(8,128)(2,1)}, u32[]{:S(2)}) copy-start(bf16[512,2048]{1,0:T(8,128)(2,1)} %all-gather.17.cloned.1.call-done) | copy-start | bytes 6291460
  241.8 5.6 copy-start.5
  247.3 1.9 copy-start.3
  247.3 1.9 copy-start.6
  247.4 2.3 copy-start.12
  253.1 1.0 copy-start.2
  253.1 29.5 %copy-start = (bf16[128,2048]{1,0:T(8,128)(2,1)S(1)}, bf16[128,2048]{1,0:T(8,128)(2,1)}, u32[]{:S(2)}) copy-start(bf16[128,2048]{1,0:T(8,128)(2,1)} %param.16) | copy-start | bytes 1572868
  253.1 56.3 %all-gather.7.cloned.1.call-start = ((), (), s32[]{:S(2)}) async-start(), calls=%async_computation.3 | async-start | bytes 2621440 | tf_op jit(solution)/shard_map/all_gather | solution.py:48
  286.7 91.2 %reduce-scatter.4.cloned.1.call-start = ((), (), s32[]{:S(2)}) async-start(), calls=%async_computation.7 | async-start | bytes 2621440 | tf_op jit(solution)/shard_map/reduce_scatter | solution.py:52
  323.2 1.1 copy-start.7
  323.2 324.3 %reduce-scatter.8.cloned.1.call-start = ((), (), s32[]{:S(2)}) async-start(), calls=%async_computation.11 | async-start | bytes 19464192 | tf_op jit(solution)/shard_map/reduce_scatter | solution.py:85
  324.3 1.7 copy-start.4
  326.0 1.7 copy-start.13
  326.0 2.0 copy-start.14
  326.0 2.4 copy-start.15
  336.7 40.6 %copy-start.11 = (f32[2048]{0:T(1024)S(1)}, f32[2048]{0:T(1024)}, u32[]{:S(2)}) copy-start(f32[2048]{0:T(1024)} %param.21) | copy-start | bytes 24580
  336.7 310.8 %copy-start.10 = (f32[256,704]{0,1:T(8,128)S(1)}, f32[256,704]{0,1:T(8,128)}, u32[]{:S(2)}) copy-start(f32[256,704]{0,1:T(8,128)} %param.18) | copy-start | bytes 2162692
  336.7 310.8 %copy-start.8 = (f32[256,704]{0,1:T(8,128)S(1)}, f32[256,704]{0,1:T(8,128)}, u32[]{:S(2)}) copy-start(f32[256,704]{0,1:T(8,128)} %param.20) | copy-start | bytes 2162692
  336.7 310.8 %copy-start.9 = (f32[256,704]{0,1:T(8,128)S(1)}, f32[256,704]{0,1:T(8,128)}, u32[]{:S(2)}) copy-start(f32[256,704]{0,1:T(8,128)} %param.19) | copy-start | bytes 2162692
Sparse Core Ops, SparseCore 0:
  11.3 25.2 all-gather.16
  38.7 59.5 all-gather.8
  100.3 57.7 all-gather.10
  159.5 20.7 all-gather.14
  182.2 59.5 all-gather.12
  253.2 29.3 reduce-scatter.5
  286.8 22.5 all-gather.6
  323.3 31.8 reduce-scatter.3
  359.2 288.2 reduce-scatter.7
where the time goes:
time: 658 us; the launch traced here: 657 us
  waiting for transfers between devices  539 us (82%)
  blocking collectives  40.6 us (6%)
  matrix products  39.4 us (6%)
  other arithmetic  20.3 us (3%)
  between operations  14 us (2%)
    reduce_scatter x1, waiting for transfers between devices, per_device(): lax.psum_scatter(jnp.concatenate([column_product(normed_all, d_gate), col...  268 us
    all_gather x1, waiting for transfers between devices, per_device(): lax.all_gather(gate_weight, 'fs', axis=0, tiled=True)  61.6 us
    all_gather x1, waiting for transfers between devices, per_device(): lax.all_gather(down_weight, 'fs', axis=0, tiled=True)  61.5 us
    all_gather x1, waiting for transfers between devices, per_device(): lax.all_gather(up_weight, 'fs', axis=0, tiled=True)  54.6 us
    psum x1, blocking collectives, per_device(): gain_sum_out = gain_sum + lax.psum(gain_part, ('fs', 'tp'))  40.6 us
    reduce_scatter x1, waiting for transfers between devices, per_device(): lax.psum_scatter((times_transposed(d_gate, gate_whole) + times_transposed...  28.3 us
    all_gather x1, waiting for transfers between devices, per_device(): normed_all = lax.all_gather(normed_e, 'tp', axis=0, tiled=True)  22.7 us
    all_gather x1, waiting for transfers between devices, per_device(): piece = lax.all_gather(normed, 'tp', axis=0, tiled=True)  22.5 us
  transfers between devices with their start and end apart: 9, of which 8 were waited for; matrix products, arithmetic and copies ran while one was open for 4% of the time, Pallas kernels for 0%

commit v1 on v0

--- a/solution.py
+++ b/solution.py
@@ -1,9 +1,20 @@
+import functools
 import jax
 import jax.numpy as jnp
 from jax import lax
 from jax.sharding import PartitionSpec as P
+from jax.lax import psum
 
 epsilon = 1e-05
+
+
+def _open_indices(message, which_axis, axis_key):
+    for i in (which_axis, axis_key):
+        message = psum(message, axis_name=i)
+    return message
+
+
+return_all_edges = functools.partial(_open_indices, which_axis="tp", axis_key="fs")
 
 
 def normalize(source, gain_f):
@@ -81,7 +92,7 @@
         - values_e * scale_e**3 * jnp.mean(values_e * scaled_grad, axis=-1, keepdims=True)
     ).astype(jnp.bfloat16)
     gain_part = jnp.sum(d_normed * values_e * scale_e, axis=0)
-    gain_sum_out = gain_sum + lax.psum(gain_part, ("fs", "tp"))
+    gain_sum_out = gain_sum + return_all_edges(gain_part)
     summed = lax.psum_scatter(
         jnp.concatenate(
             [

time: 658 us -> 657 us (level)
  blocking collectives: 40.6 us -> 27.9 us
  waiting for transfers between devices: 539 us -> 550 us
    psum x1 -> x2, blocking collectives: 40.6 us -> 27.9 us  [_open_indices(): message = psum(message, axis_name=i)]
    reduce_scatter x1, waiting for transfers between devices: 268 us -> 279 us  [per_device(): lax.psum_scatter(jnp.concatenate([column_product(normed_all, d_gate), col...]
where the time goes in v1:
time: 657 us; the launch traced here: 656 us
  waiting for transfers between devices  550 us (84%)
  matrix products  39.4 us (6%)
  blocking collectives  27.9 us (4%)
  other arithmetic  20.5 us (3%)
  between operations  14 us (2%)
    reduce_scatter x1, waiting for transfers between devices, per_device(): lax.psum_scatter(jnp.concatenate([column_product(normed_all, d_gate), col...  279 us
    all_gather x1, waiting for transfers between devices, per_device(): lax.all_gather(gate_weight, 'fs', axis=0, tiled=True)  61.6 us
    all_gather x1, waiting for transfers between devices, per_device(): lax.all_gather(down_weight, 'fs', axis=0, tiled=True)  61.5 us
    all_gather x1, waiting for transfers between devices, per_device(): lax.all_gather(up_weight, 'fs', axis=0, tiled=True)  54.6 us
    reduce_scatter x1, waiting for transfers between devices, per_device(): lax.psum_scatter((times_transposed(d_gate, gate_whole) + times_transposed...  28.3 us
    psum x2, blocking collectives, _open_indices(): message = psum(message, axis_name=i)  27.9 us
    all_gather x1, waiting for transfers between devices, per_device(): normed_all = lax.all_gather(normed_e, 'tp', axis=0, tiled=True)  22.7 us
    all_gather x1, waiting for transfers between devices, per_device(): piece = lax.all_gather(normed, 'tp', axis=0, tiled=True)  22.5 us
  transfers between devices with their start and end apart: 9, of which 8 were waited for; matrix products, arithmetic and copies ran while one was open for 4% of the time, Pallas kernels for 0%

profile of v1, /device:TPU:0, one launch (start us, length us, event | category | flops | bytes accessed | tf_op | source)
XLA Modules:
  0.0 655.9 jit_solution(357755541682923632)
XLA Ops:
  7.2 0.0 all-gather.17.cloned.1.call-start
  7.2 1.2 fusion.9
  8.5 0.7 convert_element_type.49
  9.1 2.0 fusion.11
  11.2 0.0 all-gather.17.cloned.1.call-update
  11.2 0.0 all-gather.9.cloned.1.call-start
  11.2 0.7 all-gather.9.cloned.1.call-update
  11.9 0.0 all-gather.11.cloned.1.call-start
  12.0 0.7 all-gather.11.cloned.1.call-update
  12.7 0.0 all-gather.15.cloned.1.call-start
  12.7 0.5 all-gather.15.cloned.1.call-update
  13.3 0.0 all-gather.13.cloned.1.call-start
  13.3 0.5 all-gather.13.cloned.1.call-update
  13.8 0.0 reduce-scatter.6.cloned.1.call-start
  13.9 22.7 %all-gather.17.cloned.1.call-done = bf16[512,2048]{1,0:T(8,128)(2,1)} async-done(((bf16[128,2048]{1,0:T(8,128)(2,1)}), bf16[512,2048]{1,0:T(8,128)(2,1)}) %all-gather.17.cloned.1.call-update) | async-done | bytes 2097168 | tf_op jit(solution)/shard_map/all_gather | solution.py:71
  36.6 61.6 %all-gather.9.cloned.1.call-done = bf16[2048,704]{0,1:T(8,128)(2,1)} async-done(((bf16[256,704]{0,1:T(8,128)(2,1)}), bf16[2048,704]{0,1:T(8,128)(2,1)}) %all-gather.9.cloned.1.call-update) | async-done | bytes 2883600 | tf_op jit(solution)/shard_map/all_gather | solution.py:52
  98.3 5.2 fusion.21
  103.5 54.6 %all-gather.11.cloned.1.call-done = bf16[2048,704]{0,1:T(8,128)(2,1)} async-done(((bf16[256,704]{0,1:T(8,128)(2,1)}), bf16[2048,704]{0,1:T(8,128)(2,1)}) %all-gather.11.cloned.1.call-update) | async-done | bytes 2883600 | tf_op jit(solution)/shard_map/all_gather | solution.py:53
  158.1 0.0 copy-done.1
  158.1 4.6 fusion.20
  162.7 17.6 %all-gather.15.cloned.1.call-done = bf16[512,2048]{1,0:T(8,128)(2,1)} async-done(((bf16[128,2048]{1,0:T(8,128)(2,1)}), bf16[512,2048]{1,0:T(8,128)(2,1)}) %all-gather.15.cloned.1.call-update) | async-done | bytes 2097168 | tf_op jit(solution)/shard_map/all_gather | solution.py:72
  180.3 61.5 %all-gather.13.cloned.1.call-done = bf16[2048,704]{0,1:T(8,128)(2,1)} async-done(((bf16[256,704]{0,1:T(8,128)(2,1)}), bf16[2048,704]{0,1:T(8,128)(2,1)}) %all-gather.13.cloned.1.call-update) | async-done | bytes 2883600 | tf_op jit(solution)/shard_map/all_gather | solution.py:54
  241.8 5.5 multiply_convert_fusion.1
  247.3 0.0 copy-start.3
  247.3 0.0 copy-start.6
  247.3 0.0 copy-done.5
  247.4 0.0 copy-start.12
  247.4 1.8 fusion.22
  249.2 0.0 copy-done.3
  249.2 0.0 copy-done.6
  249.2 0.5 copy-done.12
  249.7 3.4 add_convert_fusion
  253.0 0.0 reduce-scatter.6.cloned.1.call-update
  253.1 0.0 all-gather.7.cloned.1.call-start
  253.1 1.0 copy-done.2
  254.1 0.2 fusion.5
  254.3 28.3 %reduce-scatter.6.cloned.1.call-done = bf16[128,2048]{1,0:T(8,128)(2,1)} async-done(((bf16[512,2048]{1,0:T(8,128)(2,1)}), bf16[128,2048]{1,0:T(8,128)(2,1)}) %reduce-scatter.6.cloned.1.call-update) | async-done | bytes 524304 | tf_op jit(solution)/shard_map/reduce_scatter | solution.py:80
  282.6 0.0 copy-done
  282.6 1.4 fusion.15
  284.0 2.7 fusion.4
  286.6 0.0 all-gather.7.cloned.1.call-update
  286.7 0.2 reduce-scatter.4.cloned.1.call-start
  286.9 22.5 %all-gather.7.cloned.1.call-done = bf16[512,2048]{1,0:T(8,128)(2,1)} async-done(((bf16[128,2048]{1,0:T(8,128)(2,1)}), bf16[512,2048]{1,0:T(8,128)(2,1)}) %all-gather.7.cloned.1.call-update) | async-done | bytes 2097168 | tf_op jit(solution)/shard_map/all_gather | solution.py:59
  309.4 5.2 fusion.19
  314.6 8.5 %convolution_convert_fusion = bf16[512,2048]{1,0:T(8,128)(2,1)} fusion(bf16[2048,704]{0,1:T(8,128)(2,1)} %all-gather.13.cloned.1.call-done, bf16[512,2048]{1,0:T(8,128)(2,1)} %all-gather.7.cloned.1.call-done, bf16[2048,704]{0,1:T(8,128)(2,1)} %all-gather.11.cloned.1.call-done, f32[512,704]{0,1:T(8,128)} %fusion.19), kind=kOutput, calls=%fused_computation.3 | convolution fusion | flops 2956001280 | bytes 11403264 | tf_op jit(solution)/shard_map/dot_general | solution.py:27
  323.1 0.0 reduce-scatter.4.cloned.1.call-update
  323.2 0.0 reduce-scatter.8.cloned.1.call-start
  323.2 1.0 copy-done.7
  324.3 1.7 fusion.24
  325.9 0.0 copy-done.4
  326.0 1.7 fusion.23
  327.7 0.3 copy-done.14
  327.9 0.4 copy-done.15
  328.4 1.7 multiply_bitcast_fusion
  330.1 6.6 pad_maximum_fusion
  336.6 0.0 reduce-scatter.8.cloned.1.call-update
  336.7 0.0 copy-start.8
  336.7 0.0 copy-start.9
  336.7 6.1 psum.14
  342.8 21.8 %psum.15 = f32[2048]{0:T(1024)S(1)} all-reduce(f32[2048]{0:T(1024)S(1)} %psum.14), channel_id=1, replica_groups=mesh['fs'=8,'tp'=4] {'fs'}, use_global_device_ids=true, to_apply=%region_8.9 | all-reduce | flops 2048 | bytes 16384 | tf_op jit(solution)/shard_map/psum | solution.py:13
  364.6 0.6 add.71
  365.2 2.1 fusion.8
  367.4 279.0 %reduce-scatter.8.cloned.1.call-done = f32[256,2112]{0,1:T(8,128)} async-done(((f32[2048,2112]{0,1:T(8,128)}), f32[256,2112]{0,1:T(8,128)}) %reduce-scatter.8.cloned.1.call-update) | async-done | bytes 2162704 | tf_op jit(solution)/shard_map/reduce_scatter | solution.py:96
  646.4 3.0 slice_add_fusion
  (20 shorter events, 0.1 us)
Async XLA Ops:
  7.2 29.5 %all-gather.17.cloned.1.call-start = ((), (), s32[]{:S(2)}) async-start(), calls=%async_computation.9 | async-start | bytes 2621440 | tf_op jit(solution)/shard_map/all_gather | solution.py:71
  11.2 87.1 %all-gather.9.cloned.1.call-start = ((), (), s32[]{:S(2)}) async-start(), calls=%async_computation.4 | async-start | bytes 3244032 | tf_op jit(solution)/shard_map/all_gather | solution.py:52
  11.9 146.1 %all-gather.11.cloned.1.call-start = ((), (), s32[]{:S(2)}) async-start(), calls=%async_computation.5 | async-start | bytes 3244032 | tf_op jit(solution)/shard_map/all_gather | solution.py:53
  12.7 167.6 %all-gather.15.cloned.1.call-start = ((), (), s32[]{:S(2)}) async-start(), calls=%async_computation.8 | async-start | bytes 2621440 | tf_op jit(solution)/shard_map/all_gather | solution.py:72
  13.3 228.5 %all-gather.13.cloned.1.call-start = ((), (), s32[]{:S(2)}) async-start(), calls=%async_computation.6 | async-start | bytes 3244032 | tf_op jit(solution)/shard_map/all_gather | solution.py:54
  13.8 268.7 %reduce-scatter.6.cloned.1.call-start = ((), (), s32[]{:S(2)}) async-start(), calls=%async_computation.10 | async-start | bytes 2621440 | tf_op jit(solution)/shard_map/reduce_scatter | solution.py:80
  36.6 121.5 %copy-start.1 = (bf16[512,2048]{1,0:T(8,128)(2,1)S(1)}, bf16[512,2048]{1,0:T(8,128)(2,1)}, u32[]{:S(2)}) copy-start(bf16[512,2048]{1,0:T(8,128)(2,1)} %all-gather.17.cloned.1.call-done) | copy-start | bytes 6291460
  241.8 5.6 copy-start.5
  247.3 1.9 copy-start.3
  247.3 1.9 copy-start.6
  247.4 2.3 copy-start.12
  253.0 1.0 copy-start.2
  253.0 29.5 %copy-start = (bf16[128,2048]{1,0:T(8,128)(2,1)S(1)}, bf16[128,2048]{1,0:T(8,128)(2,1)}, u32[]{:S(2)}) copy-start(bf16[128,2048]{1,0:T(8,128)(2,1)} %param.16) | copy-start | bytes 1572868
  253.1 56.3 %all-gather.7.cloned.1.call-start = ((), (), s32[]{:S(2)}) async-start(), calls=%async_computation.3 | async-start | bytes 2621440 | tf_op jit(solution)/shard_map/all_gather | solution.py:59
  286.7 78.6 %reduce-scatter.4.cloned.1.call-start = ((), (), s32[]{:S(2)}) async-start(), calls=%async_computation.7 | async-start | bytes 2621440 | tf_op jit(solution)/shard_map/reduce_scatter | solution.py:63
  323.1 1.1 copy-start.7
  323.2 323.2 %reduce-scatter.8.cloned.1.call-start = ((), (), s32[]{:S(2)}) async-start(), calls=%async_computation.11 | async-start | bytes 19464192 | tf_op jit(solution)/shard_map/reduce_scatter | solution.py:96
  324.3 1.7 copy-start.4
  325.9 1.7 copy-start.13
  325.9 2.0 copy-start.14
  325.9 2.4 copy-start.15
  336.6 28.0 %copy-start.11 = (f32[2048]{0:T(1024)S(1)}, f32[2048]{0:T(1024)}, u32[]{:S(2)}) copy-start(f32[2048]{0:T(1024)} %param.21) | copy-start | bytes 24580
  336.6 309.8 %copy-start.10 = (f32[256,704]{0,1:T(8,128)S(1)}, f32[256,704]{0,1:T(8,128)}, u32[]{:S(2)}) copy-start(f32[256,704]{0,1:T(8,128)} %param.18) | copy-start | bytes 2162692
  336.7 309.8 %copy-start.8 = (f32[256,704]{0,1:T(8,128)S(1)}, f32[256,704]{0,1:T(8,128)}, u32[]{:S(2)}) copy-start(f32[256,704]{0,1:T(8,128)} %param.20) | copy-start | bytes 2162692
  336.7 309.8 %copy-start.9 = (f32[256,704]{0,1:T(8,128)S(1)}, f32[256,704]{0,1:T(8,128)}, u32[]{:S(2)}) copy-start(f32[256,704]{0,1:T(8,128)} %param.19) | copy-start | bytes 2162692
Sparse Core Ops, SparseCore 0:
  11.3 25.2 all-gather.16
  38.7 59.5 all-gather.8
  100.3 57.7 all-gather.10
  159.5 20.7 all-gather.14
  182.2 59.5 all-gather.12
  253.2 29.3 reduce-scatter.5
  286.8 22.5 all-gather.6
  323.3 31.2 reduce-scatter.3
  358.5 287.8 reduce-scatter.7
